TPU v7x, 32 devices: a whole 2x2x4 slice. The times are simulated.
32 devices in a mesh: sp: 8 (over z, x), tp: 4 (over y, core).
Axes of the slice: x: 2, y: 2, z: 4, core: 2. Of those that a mesh axis runs over, the one named last changes fastest.
Arguments:
- query_small: bfloat16 [6144, 1024], P('sp', 'tp'), may hold values from -6 to 6
- key_small: bfloat16 [6144, 1024], P('sp', 'tp'), may hold values from -6 to 6
- value_small: bfloat16 [6144, 1024], P('sp', 'tp'), may hold values from -6 to 6
- gates_small: float32 [6144, 16], P('sp', 'tp'), as said below
- query_large: bfloat16 [6144, 1024], P('sp', 'tp'), may hold values from -6 to 6
- key_large: bfloat16 [6144, 1024], P('sp', 'tp'), may hold values from -6 to 6
- value_large: bfloat16 [6144, 1024], P('sp', 'tp'), may hold values from -6 to 6
- gates_large: float32 [6144, 8], P('sp', 'tp'), as said below
- residual: bfloat16 [6144, 2048], P(('sp', 'tp')), may hold values from -6 to 6
- mixer_small: bfloat16 [1024, 2048], P('tp'), may hold values from -1 to 1
- mixer_large: bfloat16 [1024, 2048], P('tp'), may hold values from -1 to 1
- mix_gain: float32 [2048], replicated, may hold values from 0.1 to 1.9
- value_weight: bfloat16 [2048, 5632], P('sp', 'tp'), may hold values from -0.125 to 0.125
- gate_weight: bfloat16 [2048, 5632], P('sp', 'tp'), may hold values from -0.125 to 0.125
- value_taps: float32 [3, 5632], P(None, 'tp'), may hold values from -3 to 3
- gate_taps: float32 [3, 5632], P(None, 'tp'), may hold values from -3 to 3
- down_weight: bfloat16 [5632, 2048], P('tp', 'sp'), may hold values from -0.078125 to 0.078125
- final_gain: float32 [2048], replicated, may hold values from 0.1 to 1.9
Outputs:
- layer_out: bfloat16 [6144, 2048], P(('sp', 'tp'))
Inputs may be any that keep to these rules, and one draw needn't show every extreme that they name: `gates_small`: each column never rises from one position to the next, and its first entry is negative. `gates_large`: each column never rises from one position to the next, and its first entry is negative.
All inputs are finite; a program needn't handle non-finite values.
Results may differ from a plain program's by a relative error of at most 0.018.
Values may be sent and summed in bfloat16 or wider, within the bound.
A program may use at most 128 MiB of HBM per device.

v0:
```python
import math
import jax
import jax.numpy as jnp
from jax import lax
from jax.sharding import PartitionSpec as P

DS = 64
DL = 128
residual_scale = 2.0**0.5
epsilon = 1e-05


def passed_along(value, axis, steps):
    count = lax.axis_size(axis)
    first, last = (max(0, -steps), min(count, count - steps))
    return lax.ppermute(value, axis, [(source, source + steps) for source in range(first, last)])


def norm_rows(values, gain):
    center = jnp.mean(values, axis=-1, keepdims=True)
    spread = jnp.mean(jnp.square(values - center), axis=-1, keepdims=True)
    return (values - center) * lax.rsqrt(spread + epsilon) * gain


def attend_block(
    running,
    queries,
    query_gates,
    key_rows,
    value_rows,
    key_gates,
    token_positions,
    key_first,
    head_dim,
):
    running_peak, weight_sum, weighted = running
    heads_here = query_gates.shape[1]
    span_rows = key_rows.shape[0]
    query_heads = queries.reshape(queries.shape[0], heads_here, head_dim)
    key_heads = key_rows.reshape(span_rows, heads_here, head_dim)
    value_heads = value_rows.reshape(span_rows, heads_here, head_dim)
    scores = jnp.einsum(
        "qhd,khd->hqk", query_heads, key_heads, preferred_element_type=jnp.float32
    ) * head_dim ** (-0.5)
    scores = scores + query_gates.T[:, :, None] - key_gates.T[:, None, :]
    key_positions = key_first + jnp.arange(span_rows)
    allowed = token_positions[:, None] >= key_positions[None, :]
    scores = jnp.where(allowed[None], scores, -1e30)
    new_peak = jnp.maximum(running_peak, jnp.max(scores, axis=-1))
    factor = jnp.exp(running_peak - new_peak)
    weights = jnp.where(allowed[None], jnp.exp(scores - new_peak[:, :, None]), 0.0)
    weight_sum = weight_sum * factor + jnp.sum(weights, axis=-1)
    update = jnp.einsum(
        "hqk,khd->qhd",
        weights.astype(jnp.bfloat16),
        value_heads,
        preferred_element_type=jnp.float32,
    )
    weighted = weighted * factor.T[:, :, None] + update
    return (new_peak, weight_sum, weighted)


def per_device(
    query_small,
    key_small,
    value_small,
    gates_small,
    query_large,
    key_large,
    value_large,
    gates_large,
    residual,
    mixer_small,
    mixer_large,
    mix_gain,
    value_weight,
    gate_weight,
    value_taps,
    gate_taps,
    down_weight,
    final_gain,
):
    shard_rows = query_small.shape[0]
    first_row = lax.axis_index("sp") * shard_rows
    token_positions = first_row + jnp.arange(shard_rows)
    last_position = first_row + shard_rows - 1
    every_gate = (
        lax.all_gather(gates_small, "sp", axis=0, tiled=True),
        lax.all_gather(gates_large, "sp", axis=0, tiled=True),
    )
    heads_small = gates_small.shape[1]
    heads_large = gates_large.shape[1]

    def fresh(heads_here, head_dim):
        return (
            jnp.full((heads_here, shard_rows), -1e30, jnp.float32),
            jnp.zeros((heads_here, shard_rows), jnp.float32),
            jnp.zeros((shard_rows, heads_here, head_dim), jnp.float32),
        )

    pieces = (
        lax.all_gather(key_small, "sp", axis=0, tiled=True),
        lax.all_gather(value_small, "sp", axis=0, tiled=True),
        lax.all_gather(key_large, "sp", axis=0, tiled=True),
        lax.all_gather(value_large, "sp", axis=0, tiled=True),
    )
    span_total = pieces[0].shape[0]
    block_rows = shard_rows * math.gcd(span_total // shard_rows, max(1, 1024 // shard_rows))

    def one_block(block_index, current):
        offset = block_index * block_rows
        sliced = [lax.dynamic_slice_in_dim(member, offset, block_rows, 0) for member in pieces]
        gate_small = lax.dynamic_slice_in_dim(every_gate[0], offset, block_rows, 0)
        gate_large = lax.dynamic_slice_in_dim(every_gate[1], offset, block_rows, 0)

        def update(previous):
            return (
                attend_block(
                    previous[0],
                    query_small,
                    gates_small,
                    sliced[0],
                    sliced[1],
                    gate_small,
                    token_positions,
                    offset,
                    DS,
                ),
                attend_block(
                    previous[1],
                    query_large,
                    gates_large,
                    sliced[2],
                    sliced[3],
                    gate_large,
                    token_positions,
                    offset,
                    DL,
                ),
            )

        def unchanged(previous):
            return previous

        return lax.cond(offset <= last_position, update, unchanged, current)

    block_count = span_total // block_rows
    small_state, large_state = lax.fori_loop(
        0, block_count, one_block, (fresh(heads_small, DS), fresh(heads_large, DL))
    )
    small_out = (
        (small_state[2] / small_state[1].T[:, :, None])
        .reshape(shard_rows, heads_small * DS)
        .astype(jnp.bfloat16)
    )
    large_out = (
        (large_state[2] / large_state[1].T[:, :, None])
        .reshape(shard_rows, heads_large * DL)
        .astype(jnp.bfloat16)
    )
    tensor_parts = lax.axis_size("tp")
    own_rows = shard_rows // tensor_parts
    joined = jnp.concatenate([small_out, large_out], axis=1)
    arrived = lax.all_to_all(joined, "tp", split_axis=0, concat_axis=1, tiled=True)
    layout = arrived.reshape(own_rows, tensor_parts, joined.shape[1])
    small_width = small_out.shape[1]
    all_small = layout[:, :, :small_width].reshape(own_rows, tensor_parts * small_width)
    all_large = layout[:, :, small_width:].reshape(own_rows, tensor_parts * large_out.shape[1])
    mix = jnp.dot(
        all_small,
        lax.all_gather(mixer_small, "tp", axis=0, tiled=True),
        preferred_element_type=jnp.float32,
    ) + jnp.dot(
        all_large,
        lax.all_gather(mixer_large, "tp", axis=0, tiled=True),
        preferred_element_type=jnp.float32,
    )
    mixed = norm_rows(residual_scale * residual.astype(jnp.float32) + mix, mix_gain).astype(
        jnp.bfloat16
    )
    block_input = lax.all_gather(mixed, "tp", axis=0, tiled=True)

    def add_up(pieces):
        return (
            jnp.dot(block_input, pieces[0], preferred_element_type=jnp.float32),
            jnp.dot(block_input, pieces[1], preferred_element_type=jnp.float32),
        )

    up_value, up_gate = add_up(
        (
            lax.all_gather(value_weight, "sp", axis=0, tiled=True),
            lax.all_gather(gate_weight, "sp", axis=0, tiled=True),
        )
    )
    up_value = up_value.astype(jnp.bfloat16)
    up_gate = up_gate.astype(jnp.bfloat16)
    hidden_width = up_value.shape[1]
    trailing = jnp.concatenate([up_value[-2:], up_gate[-2:]], axis=1)
    earlier = passed_along(trailing, "sp", 1)
    padded_value = jnp.concatenate([earlier[:, :hidden_width], up_value], axis=0).astype(
        jnp.float32
    )
    padded_gate = jnp.concatenate([earlier[:, hidden_width:], up_gate], axis=0).astype(jnp.float32)
    filt_value = (
        value_taps[0] * padded_value[:-2]
        + value_taps[1] * padded_value[1:-1]
        + value_taps[2] * padded_value[2:]
    )
    filt_gate = (
        gate_taps[0] * padded_gate[:-2]
        + gate_taps[1] * padded_gate[1:-1]
        + gate_taps[2] * padded_gate[2:]
    )
    hidden = (jax.nn.silu(filt_gate) * filt_value).astype(jnp.bfloat16)
    ffn_terms = jnp.dot(
        hidden,
        lax.all_gather(down_weight, "sp", axis=1, tiled=True),
        preferred_element_type=jnp.float32,
    )
    ffn = lax.psum_scatter(
        ffn_terms.astype(jnp.bfloat16), "tp", scatter_dimension=0, tiled=True
    ).astype(jnp.float32)
    return norm_rows(residual_scale * mixed.astype(jnp.float32) + ffn, final_gain).astype(
        jnp.bfloat16
    )


def solution(mesh):
    in_specs = (
        P("sp", "tp"),
        P("sp", "tp"),
        P("sp", "tp"),
        P("sp", "tp"),
        P("sp", "tp"),
        P("sp", "tp"),
        P("sp", "tp"),
        P("sp", "tp"),
        P(("sp", "tp"), None),
        P("tp", None),
        P("tp", None),
        P(),
        P("sp", "tp"),
        P("sp", "tp"),
        P(None, "tp"),
        P(None, "tp"),
        P("tp", "sp"),
        P(),
    )
    out_specs = P(("sp", "tp"), None)
    return jax.shard_map(
        per_device, mesh=mesh, in_specs=in_specs, out_specs=out_specs, check_vma=False
    )
```

profile of v0, /device:TPU:0, one launch (start us, length us, event | category | flops | bytes accessed | tf_op | source)
XLA Modules:
  0.0 712.8 jit_solution(5404534390486293177)
XLA Ops:
  16.8 33.1 %all_gather.40 = f32[6144,2]{0,1:T(2,128)S(1)} all-gather(f32[768,2]{0,1:T(2,128)S(1)} %copy-done.5), channel_id=1, replica_groups=mesh['sp'=8,'tp'=4] {'sp'}, dimensions={0}, use_global_device_ids=true | all-gather | bytes 55296 | tf_op jit(solution)/shard_map/all_gather | solution.py:89
  49.9 31.3 %all_gather.37 = f32[6144,4]{0,1:T(4,128)S(1)} all-gather(f32[768,4]{0,1:T(4,128)S(1)} %copy-done.3), channel_id=1, replica_groups=mesh['sp'=8,'tp'=4] {'sp'}, dimensions={0}, use_global_device_ids=true | all-gather | bytes 110592 | tf_op jit(solution)/shard_map/all_gather | solution.py:88
  81.2 53.8 %all-gather.13.cloned.1.call-done = bf16[6144,256]{0,1:T(8,128)(2,1)} async-done(((bf16[768,256]{0,1:T(8,128)(2,1)}), bf16[6144,256]{0,1:T(8,128)(2,1)}) %all-gather.13.cloned.1.call-update) | async-done | bytes 3145744 | tf_op jit(solution)/shard_map/all_gather | solution.py:103
  135.0 61.0 %all-gather.15.cloned.1.call-done = bf16[6144,256]{0,1:T(8,128)(2,1)} async-done(((bf16[768,256]{0,1:T(8,128)(2,1)}), bf16[6144,256]{0,1:T(8,128)(2,1)}) %all-gather.15.cloned.1.call-update) | async-done | bytes 3145744 | tf_op jit(solution)/shard_map/all_gather | solution.py:104
  196.0 60.8 %all-gather.17.cloned.1.call-done = bf16[6144,256]{0,1:T(8,128)(2,1)} async-done(((bf16[768,256]{0,1:T(8,128)(2,1)}), bf16[6144,256]{0,1:T(8,128)(2,1)}) %all-gather.17.cloned.1.call-update) | async-done | bytes 3145744 | tf_op jit(solution)/shard_map/all_gather | solution.py:105
  257.0 19.2 %while.24 = (s32[]{:T(128)}, f32[4,768]{1,0:T(4,128)S(1)}, f32[4,768]{1,0:T(4,128)S(1)}, f32[768,4,64]{0,2,1:T(8,128)S(1)}, f32[2,768]{1,0:T(2,128)S(1)}, /*inde...) while((s32[]{:T(128)}, f32[4,768]{1,0:T(4,128)S(1)}, ...), condition=%wide.region_7.8_spmd.clone, body=%wide.region_0.7_spmd.clone.sunk | while | flops 1276591104 | bytes 55708176 | solution.py:148
  257.0 18.5 %conditional.3 = ((f32[4,768]{1,0:T(4,128)S(1)}, f32[4,768]{1,0:T(4,128)S(1)}, f32[768,4,64]{0,2,1:T(8,128)S(1)}, f32[2,768]{1,0:T(2,128)S(1)}, f32[2,768]{1,0:T(2,128)S(1)}, /*index=5*/f32[768,2,128]{2,0,1:T(8,128)S(1)})) conditional(s32[]{:T(128)} %convert_element_type.127, (f32[4,768]{1,0:T(4,128)S(1)}, f32[4,768]{1,0:T(4,128)S(1)}, ...), branch_computations={%region_1.0_spmd, %region_2.6_spmd} | conditional | flops 1276591104 | bytes 55704688 | solution.py:145
  260.2 2.5 fusion.20
  265.7 2.7 fusion.4
  268.5 3.6 fusion.23
  272.1 3.5 fusion.3
  279.1 19.0 %all_to_all.13 = bf16[4,192,512]{2,1,0:T(8,128)(2,1)S(1)} all-to-all(bf16[4,192,512]{2,1,0:T(8,128)(2,1)S(1)} %copy.51), channel_id=1, replica_groups=mesh['sp'=8,'tp'=4] {'tp'}, dimensions={0} | all-to-all | bytes 1572864 | tf_op jit(solution)/shard_map/all_to_all | solution.py:164
  298.3 3.5 fusion.49
  301.8 26.2 %all-gather.21.cloned.1.call-done = bf16[1024,2048]{1,0:T(8,128)(2,1)} async-done(((bf16[256,2048]{1,0:T(8,128)(2,1)}), bf16[1024,2048]{1,0:T(8,128)(2,1)}) %all-gather.21.cloned.1.call-update) | async-done | bytes 4194320 | tf_op jit(solution)/shard_map/all_gather | solution.py:175
  328.0 3.6 fusion.48
  334.5 92.2 %all-gather.25.cloned.1.call-done = bf16[2048,1408]{1,0:T(8,128)(2,1)} async-done(((bf16[256,1408]{1,0:T(8,128)(2,1)}), bf16[2048,1408]{1,0:T(8,128)(2,1)}) %all-gather.25.cloned.1.call-update) | async-done | bytes 5767184 | tf_op jit(solution)/shard_map/all_gather | solution.py:191
  426.7 30.9 %all-gather.23.cloned.1.call-done = bf16[768,2048]{1,0:T(8,128)(2,1)} async-done(((bf16[192,2048]{1,0:T(8,128)(2,1)}), bf16[768,2048]{1,0:T(8,128)(2,1)}) %all-gather.23.cloned.1.call-update) | async-done | bytes 3145744 | tf_op jit(solution)/shard_map/all_gather | solution.py:181
  457.6 8.3 %convolution_convert_fusion.2 = bf16[768,1408]{1,0:T(8,128)(2,1)S(1)} fusion(bf16[768,2048]{1,0:T(8,128)(2,1)} %all-gather.23.cloned.1.call-done, bf16[2048,1408]{1,0:T(8,128)(2,1)} %all-gather.25.cloned.1.call-done), kind=kOutput, calls=%fused_computation.57 | convolution fusion | flops 4430266368 | bytes 11075584 | tf_op jit(solution)/shard_map/dot_general | solution.py:185
  467.3 84.8 %all-gather.27.cloned.1.call-done = bf16[2048,1408]{1,0:T(8,128)(2,1)} async-done(((bf16[256,1408]{1,0:T(8,128)(2,1)}), bf16[2048,1408]{1,0:T(8,128)(2,1)}) %all-gather.27.cloned.1.call-update) | async-done | bytes 5767184 | tf_op jit(solution)/shard_map/all_gather | solution.py:192
  552.1 8.5 %convolution_convert_fusion.1 = bf16[768,1408]{1,0:T(8,128)(2,1)S(1)} fusion(bf16[768,2048]{1,0:T(8,128)(2,1)} %all-gather.23.cloned.1.call-done, bf16[2048,1408]{1,0:T(8,128)(2,1)} %all-gather.27.cloned.1.call-done), kind=kOutput, calls=%fused_computation.56 | convolution fusion | flops 4430266368 | bytes 11075584 | tf_op jit(solution)/shard_map/dot_general | solution.py:186
  564.6 4.2 maximum_convert_fusion
  568.9 76.7 %all-gather.29.cloned.1.call-done = bf16[1408,2048]{1,0:T(8,128)(2,1)} async-done(((bf16[1408,256]{1,0:T(8,128)(2,1)}), bf16[1408,2048]{1,0:T(8,128)(2,1)}) %all-gather.29.cloned.1.call-update) | async-done | bytes 5767184 | tf_op jit(solution)/shard_map/all_gather | solution.py:217
  645.6 19.1 %convolution_convert_fusion = bf16[768,2048]{1,0:T(8,128)(2,1)} fusion(bf16[1408,2048]{1,0:T(8,128)(2,1)} %all-gather.29.cloned.1.call-done, f32[770,1408]{1,0:T(8,128)} %get-tuple-element.726, f32[770,1408]{1,0:T(8,128)} %get-tuple-element.725, f32[1408]{0:T(1024)S(1)} %get-tuple-element.665, f32[1408]{0:T(1024)S(1)} %get-tuple-element.666, ...), kind=kOutput, calls=%fused_computation.55 | convolution fusion | flops 4448059392 | bytes 34898944 | tf_op jit(solution)/shard_map/dot_general | solution.py:215
  664.7 36.2 %reduce-scatter.2.cloned.1.call-done = bf16[192,2048]{1,0:T(8,128)(2,1)} async-done(((bf16[768,2048]{1,0:T(8,128)(2,1)}), bf16[192,2048]{1,0:T(8,128)(2,1)}) %reduce-scatter.2.cloned.1.call-update) | async-done | bytes 786448 | tf_op jit(solution)/shard_map/reduce_scatter | solution.py:220
  (112 shorter events, 33.0 us)
Async XLA Ops:
  6.5 10.1 %copy-start.4 = (bf16[768,256]{1,0:T(8,128)(2,1)S(1)}, bf16[768,256]{1,0:T(8,128)(2,1)}, u32[]{:S(2)}) copy-start(bf16[768,256]{1,0:T(8,128)(2,1)} %param.22) | copy-start | bytes 1179652
  6.5 10.2 %copy-start.5 = (f32[768,2]{0,1:T(2,128)S(1)}, f32[768,2]{0,1:T(2,128)}, u32[]{:S(2)}) copy-start(f32[768,2]{0,1:T(2,128)} %param.29) | copy-start | bytes 18436
  6.5 43.4 %copy-start.3 = (f32[768,4]{0,1:T(4,128)S(1)}, f32[768,4]{0,1:T(4,128)}, u32[]{:S(2)}) copy-start(f32[768,4]{0,1:T(4,128)} %param.25) | copy-start | bytes 36868
  6.5 74.7 %all-gather.11.cloned.1.call-start = ((), (), s32[]{:S(2)}) async-start(), calls=%async_computation.2 | async-start | bytes 3538944 | tf_op jit(solution)/shard_map/all_gather | solution.py:102
  8.5 248.5 %copy-start.10 = (bf16[768,256]{1,0:T(8,128)(2,1)S(1)}, bf16[768,256]{1,0:T(8,128)(2,1)}, u32[]{:S(2)}) copy-start(bf16[768,256]{1,0:T(8,128)(2,1)} %param.26) | copy-start | bytes 1179652
  8.5 126.5 %all-gather.13.cloned.1.call-start = ((), (), s32[]{:S(2)}) async-start(), calls=%async_computation.3 | async-start | bytes 3538944 | tf_op jit(solution)/shard_map/all_gather | solution.py:103
  10.6 185.4 %all-gather.15.cloned.1.call-start = ((), (), s32[]{:S(2)}) async-start(), calls=%async_computation.4 | async-start | bytes 3538944 | tf_op jit(solution)/shard_map/all_gather | solution.py:104
  12.6 244.2 %all-gather.17.cloned.1.call-start = ((), (), s32[]{:S(2)}) async-start(), calls=%async_computation.5 | async-start | bytes 3538944 | tf_op jit(solution)/shard_map/all_gather | solution.py:105
  14.6 283.6 %all-gather.19.cloned.1.call-start = ((), (), s32[]{:S(2)}) async-start(), calls=%async_computation.6 | async-start | bytes 5242880 | tf_op jit(solution)/shard_map/all_gather | solution.py:171
  15.2 312.8 %all-gather.21.cloned.1.call-start = ((), (), s32[]{:S(2)}) async-start(), calls=%async_computation.7 | async-start | bytes 5242880 | tf_op jit(solution)/shard_map/all_gather | solution.py:175
  15.8 410.9 %all-gather.25.cloned.1.call-start = ((), (), s32[]{:S(2)}) async-start(), calls=%async_computation.9 | async-start | bytes 6488064 | tf_op jit(solution)/shard_map/all_gather | solution.py:191
  16.5 441.0 %all-gather.23.cloned.1.call-start = ((), (), s32[]{:S(2)}) async-start(), calls=%async_computation.8 | async-start | bytes 3932160 | tf_op jit(solution)/shard_map/all_gather | solution.py:181
  328.0 3.9 copy-start.6
  333.1 218.9 %all-gather.27.cloned.1.call-start = ((), (), s32[]{:S(2)}) async-start(), calls=%async_computation.10 | async-start | bytes 6488064 | tf_op jit(solution)/shard_map/all_gather | solution.py:192
  333.9 311.7 %all-gather.29.cloned.1.call-start = ((), (), s32[]{:S(2)}) async-start(), calls=%async_computation.11 | async-start | bytes 6488064 | tf_op jit(solution)/shard_map/all_gather | solution.py:217
  334.5 366.5 %reduce-scatter.2.cloned.1.call-start = ((), (), s32[]{:S(2)}) async-start(), calls=%async_computation.12 | async-start | bytes 3932160 | tf_op jit(solution)/shard_map/reduce_scatter | solution.py:220
  465.9 1.4 copy-start.1
  467.3 95.8 %copy-start.7 = (f32[3,1408]{1,0:T(4,128)S(1)}, f32[3,1408]{1,0:T(4,128)}, u32[]{:S(2)}) copy-start(f32[3,1408]{1,0:T(4,128)} %param.36) | copy-start | bytes 50692
  467.3 95.8 %copy-start.8 = (f32[3,1408]{1,0:T(4,128)S(1)}, f32[3,1408]{1,0:T(4,128)}, u32[]{:S(2)}) copy-start(f32[3,1408]{1,0:T(4,128)} %param.37) | copy-start | bytes 50692
  552.1 12.6 %copy-start.2 = (bf16[768,1408]{1,0:T(8,128)(2,1)S(1)}, bf16[768,1408]{1,0:T(8,128)(2,1)}, u32[]{:S(2)}) copy-start(bf16[768,1408]{1,0:T(8,128)(2,1)} %copy-done.1) | copy-start | bytes 6488068
  560.6 4.0 collective-permute-start
  664.7 39.7 %copy-start.9 = (f32[2048]{0:T(1024)S(1)}, f32[2048]{0:T(1024)}, u32[]{:S(2)}) copy-start(f32[2048]{0:T(1024)} %param.39) | copy-start | bytes 24580
  700.9 3.5 copy-start
Sparse Core Ops, SparseCore 0:
  9.6 64.2 all-gather.10
  76.1 58.8 all-gather.12
  137.3 58.6 all-gather.14
  198.1 58.6 all-gather.16
  258.2 37.8 all-gather.18
  297.5 30.4 all-gather.20
  330.2 96.4 all-gather.24
  428.2 29.2 all-gather.22
  459.7 92.2 all-gather.26
  554.0 91.6 all-gather.28
  664.8 36.0 reduce-scatter.1
where the time goes:
time: 714 us; the launch traced here: 713 us
  waiting for transfers between devices  527 us (74%)
  blocking collectives  83.4 us (12%)
  matrix products  53.3 us (7%)
  other arithmetic  17.8 us (2%)
  local copies, waits for them, and re-layouts  14 us (2%)
  between operations  13.6 us (2%)
    all_gather x1, waiting for transfers between devices, per_device(): lax.all_gather(value_weight, 'sp', axis=0, tiled=True)  92.2 us
    all_gather x1, waiting for transfers between devices, per_device(): lax.all_gather(gate_weight, 'sp', axis=0, tiled=True)  84.8 us
    all_gather x1, waiting for transfers between devices, per_device(): lax.all_gather(down_weight, 'sp', axis=1, tiled=True)  76.7 us
    all_gather x1, waiting for transfers between devices, per_device(): lax.all_gather(key_large, 'sp', axis=0, tiled=True)  61 us
    all_gather x1, waiting for transfers between devices, per_device(): lax.all_gather(value_large, 'sp', axis=0, tiled=True)  60.8 us
    all_gather x1, waiting for transfers between devices, per_device(): lax.all_gather(value_small, 'sp', axis=0, tiled=True)  53.8 us
    reduce_scatter x1, waiting for transfers between devices, per_device(): lax.psum_scatter(ffn_terms.astype(jnp.bfloat16), 'tp', scatter_dimension=...  36.2 us
    all_gather x1, blocking collectives, per_device(): lax.all_gather(gates_large, 'sp', axis=0, tiled=True)  33.1 us
  transfers between devices with their start and end apart: 12, of which 10 were waited for; matrix products, arithmetic and copies ran while one was open for 8% of the time, Pallas kernels for 0%

commit v1 on v0

--- a/solution.py
+++ b/solution.py
@@ -214,7 +214,7 @@
     hidden = (jax.nn.silu(filt_gate) * filt_value).astype(jnp.bfloat16)
     ffn_terms = jnp.dot(
         hidden,
-        lax.all_gather(down_weight, "sp", axis=1, tiled=True),
+        jnp.concatenate(lax.all_gather(down_weight, "sp"), axis=1),
         preferred_element_type=jnp.float32,
     )
     ffn = lax.psum_scatter(

time: 714 us -> 726 us (1.017)
  local copies, waits for them, and re-layouts: 14 us -> 23.6 us
    reshape x0 -> x1, local copies, waits for them, and re-layouts: none -> 8.26 us  [per_device(): jnp.concatenate(lax.all_gather(down_weight, 'sp'), axis=1)]
  transfers between devices with their start and end apart: 12 -> 12, of which waited for: 10 -> 9; matrix products, arithmetic and copies ran while one was open for 8% -> 8% of each run, Pallas kernels for 0% -> 0%
where the time goes in v1:
time: 726 us; the launch traced here: 725 us
  waiting for transfers between devices  529 us (73%)
  blocking collectives  83.4 us (11%)
  matrix products  51.9 us (7%)
  local copies, waits for them, and re-layouts  23.6 us (3%)
  other arithmetic  20.1 us (3%)
  between operations  13.6 us (2%)
    all_gather x1, waiting for transfers between devices, per_device(): lax.all_gather(value_weight, 'sp', axis=0, tiled=True)  92.1 us
    all_gather x1, waiting for transfers between devices, per_device(): lax.all_gather(gate_weight, 'sp', axis=0, tiled=True)  84.8 us
    all_gather x1, waiting for transfers between devices, per_device(): lax.all_gather(down_weight, 'sp')  80.5 us
    all_gather x1, waiting for transfers between devices, per_device(): lax.all_gather(key_large, 'sp', axis=0, tiled=True)  61 us
    all_gather x1, waiting for transfers between devices, per_device(): lax.all_gather(value_large, 'sp', axis=0, tiled=True)  60.8 us
    all_gather x1, waiting for transfers between devices, per_device(): lax.all_gather(value_small, 'sp', axis=0, tiled=True)  53.8 us
    reduce_scatter x1, waiting for transfers between devices, per_device(): lax.psum_scatter(ffn_terms.astype(jnp.bfloat16), 'tp', scatter_dimension=...  36.2 us
    all_gather x1, blocking collectives, per_device(): lax.all_gather(gates_large, 'sp', axis=0, tiled=True)  33.1 us
  transfers between devices with their start and end apart: 12, of which 9 were waited for; matrix products, arithmetic and copies ran while one was open for 8% of the time, Pallas kernels for 0%

profile of v1, /device:TPU:0, one launch (start us, length us, event | category | flops | bytes accessed | tf_op | source)
XLA Modules:
  0.0 725.4 jit_solution(9451373479399422481)
XLA Ops:
  16.8 33.1 %all_gather.43 = f32[6144,2]{0,1:T(2,128)S(1)} all-gather(f32[768,2]{0,1:T(2,128)S(1)} %copy-done.5), channel_id=1, replica_groups=mesh['sp'=8,'tp'=4] {'sp'}, dimensions={0}, use_global_device_ids=true | all-gather | bytes 55296 | tf_op jit(solution)/shard_map/all_gather | solution.py:89
  49.9 31.3 %all_gather.40 = f32[6144,4]{0,1:T(4,128)S(1)} all-gather(f32[768,4]{0,1:T(4,128)S(1)} %copy-done.3), channel_id=1, replica_groups=mesh['sp'=8,'tp'=4] {'sp'}, dimensions={0}, use_global_device_ids=true | all-gather | bytes 110592 | tf_op jit(solution)/shard_map/all_gather | solution.py:88
  81.2 53.8 %all-gather.14.cloned.1.call-done = bf16[6144,256]{0,1:T(8,128)(2,1)} async-done(((bf16[768,256]{0,1:T(8,128)(2,1)}), bf16[6144,256]{0,1:T(8,128)(2,1)}) %all-gather.14.cloned.1.call-update) | async-done | bytes 3145744 | tf_op jit(solution)/shard_map/all_gather | solution.py:103
  135.0 61.0 %all-gather.16.cloned.1.call-done = bf16[6144,256]{0,1:T(8,128)(2,1)} async-done(((bf16[768,256]{0,1:T(8,128)(2,1)}), bf16[6144,256]{0,1:T(8,128)(2,1)}) %all-gather.16.cloned.1.call-update) | async-done | bytes 3145744 | tf_op jit(solution)/shard_map/all_gather | solution.py:104
  196.0 60.8 %all-gather.18.cloned.1.call-done = bf16[6144,256]{0,1:T(8,128)(2,1)} async-done(((bf16[768,256]{0,1:T(8,128)(2,1)}), bf16[6144,256]{0,1:T(8,128)(2,1)}) %all-gather.18.cloned.1.call-update) | async-done | bytes 3145744 | tf_op jit(solution)/shard_map/all_gather | solution.py:105
  257.0 19.2 %while.24 = (s32[]{:T(128)}, f32[4,768]{1,0:T(4,128)S(1)}, f32[4,768]{1,0:T(4,128)S(1)}, f32[768,4,64]{0,2,1:T(8,128)S(1)}, f32[2,768]{1,0:T(2,128)S(1)}, /*inde...) while((s32[]{:T(128)}, f32[4,768]{1,0:T(4,128)S(1)}, ...), condition=%wide.region_7.8_spmd.clone, body=%wide.region_0.7_spmd.clone.sunk | while | flops 1276591104 | bytes 55708176 | solution.py:148
  257.0 18.5 %conditional.3 = ((f32[4,768]{1,0:T(4,128)S(1)}, f32[4,768]{1,0:T(4,128)S(1)}, f32[768,4,64]{0,2,1:T(8,128)S(1)}, f32[2,768]{1,0:T(2,128)S(1)}, f32[2,768]{1,0:T(2,128)S(1)}, /*index=5*/f32[768,2,128]{2,0,1:T(8,128)S(1)})) conditional(s32[]{:T(128)} %convert_element_type.127, (f32[4,768]{1,0:T(4,128)S(1)}, f32[4,768]{1,0:T(4,128)S(1)}, ...), branch_computations={%region_1.0_spmd, %region_2.6_spmd} | conditional | flops 1276591104 | bytes 55704688 | solution.py:145
  265.7 2.7 fusion.4
  268.5 3.6 fusion.23
  272.1 3.5 fusion.3
  279.1 19.0 %all_to_all.13 = bf16[4,192,512]{2,1,0:T(8,128)(2,1)S(1)} all-to-all(bf16[4,192,512]{2,1,0:T(8,128)(2,1)S(1)} %copy.66), channel_id=1, replica_groups=mesh['sp'=8,'tp'=4] {'tp'}, dimensions={0} | all-to-all | bytes 1572864 | tf_op jit(solution)/shard_map/all_to_all | solution.py:164
  298.3 3.5 fusion.49
  301.8 26.3 %all-gather.22.cloned.1.call-done = bf16[1024,2048]{1,0:T(8,128)(2,1)} async-done(((bf16[256,2048]{1,0:T(8,128)(2,1)}), bf16[1024,2048]{1,0:T(8,128)(2,1)}) %all-gather.22.cloned.1.call-update) | async-done | bytes 4194320 | tf_op jit(solution)/shard_map/all_gather | solution.py:175
  328.0 3.6 fusion.48
  334.5 92.1 %all-gather.26.cloned.1.call-done = bf16[2048,1408]{1,0:T(8,128)(2,1)} async-done(((bf16[256,1408]{1,0:T(8,128)(2,1)}), bf16[2048,1408]{1,0:T(8,128)(2,1)}) %all-gather.26.cloned.1.call-update) | async-done | bytes 5767184 | tf_op jit(solution)/shard_map/all_gather | solution.py:191
  426.7 30.8 %all-gather.24.cloned.1.call-done = bf16[768,2048]{1,0:T(8,128)(2,1)} async-done(((bf16[192,2048]{1,0:T(8,128)(2,1)}), bf16[768,2048]{1,0:T(8,128)(2,1)}) %all-gather.24.cloned.1.call-update) | async-done | bytes 3145744 | tf_op jit(solution)/shard_map/all_gather | solution.py:181
  457.4 8.3 %convolution_convert_fusion.2 = bf16[768,1408]{1,0:T(8,128)(2,1)S(1)} fusion(bf16[768,2048]{1,0:T(8,128)(2,1)} %all-gather.24.cloned.1.call-done, bf16[2048,1408]{1,0:T(8,128)(2,1)} %all-gather.26.cloned.1.call-done), kind=kOutput, calls=%fused_computation.57 | convolution fusion | flops 4430266368 | bytes 11075584 | tf_op jit(solution)/shard_map/dot_general | solution.py:185
  467.2 84.8 %all-gather.28.cloned.1.call-done = bf16[2048,1408]{1,0:T(8,128)(2,1)} async-done(((bf16[256,1408]{1,0:T(8,128)(2,1)}), bf16[2048,1408]{1,0:T(8,128)(2,1)}) %all-gather.28.cloned.1.call-update) | async-done | bytes 5767184 | tf_op jit(solution)/shard_map/all_gather | solution.py:192
  552.0 8.3 %convolution_convert_fusion.1 = bf16[768,1408]{1,0:T(8,128)(2,1)S(1)} fusion(bf16[768,2048]{1,0:T(8,128)(2,1)} %all-gather.24.cloned.1.call-done, bf16[2048,1408]{1,0:T(8,128)(2,1)} %all-gather.28.cloned.1.call-done), kind=kOutput, calls=%fused_computation.56 | convolution fusion | flops 4430266368 | bytes 11075584 | tf_op jit(solution)/shard_map/dot_general | solution.py:186
  564.3 80.5 %all-gather.30.cloned.1.call-done = bf16[11264,256]{1,0:T(8,128)(2,1)} async-done(((bf16[1408,256]{1,0:T(8,128)(2,1)}), bf16[11264,256]{1,0:T(8,128)(2,1)}) %all-gather.30.cloned.1.call-update) | async-done | bytes 5767184 | tf_op jit(solution)/shard_map/all_gather | solution.py:217
  644.8 8.3 %copy.69 = bf16[1408,8,256]{0,2,1:T(8,128)(2,1)} copy(bf16[1408,8,256]{2,0,1:T(8,128)(2,1)} %bitcast.93) | data formatting | bytes 11534336 | tf_op jit(solution)/shard_map/reshape | solution.py:217
  653.0 6.5 maximum_convert_fusion
  659.6 17.7 %convolution_convert_fusion = bf16[768,2048]{1,0:T(8,128)(2,1)} fusion(bf16[1408,2048]{0,1:T(8,128)(2,1)} %bitcast.94, f32[770,1408]{1,0:T(8,128)} %get-tuple-element.745, f32[770,1408]{1,0:T(8,128)} %get-tuple-element.744, f32[1408]{0:T(1024)S(1)} %get-tuple-element.684, f32[1408]{0:T(1024)S(1)} %get-tuple-element.685, f32[1408]{0:T(1024)S(1)} %get-tuple-element.683, ...), kind=kOutput, calls=%fused_computation.55 | convolution fusion | flops 4448059392 | bytes 34898944 | tf_op jit(solution)/shard_map/dot_general | solution.py:215
  677.3 36.2 %reduce-scatter.2.cloned.1.call-done = bf16[192,2048]{1,0:T(8,128)(2,1)} async-done(((bf16[768,2048]{1,0:T(8,128)(2,1)}), bf16[192,2048]{1,0:T(8,128)(2,1)}) %reduce-scatter.2.cloned.1.call-update) | async-done | bytes 786448 | tf_op jit(solution)/shard_map/reduce_scatter | solution.py:220
  (113 shorter events, 35.5 us)
Async XLA Ops:
  6.5 10.1 %copy-start.4 = (bf16[768,256]{1,0:T(8,128)(2,1)S(1)}, bf16[768,256]{1,0:T(8,128)(2,1)}, u32[]{:S(2)}) copy-start(bf16[768,256]{1,0:T(8,128)(2,1)} %param.22) | copy-start | bytes 1179652
  6.5 10.2 %copy-start.5 = (f32[768,2]{0,1:T(2,128)S(1)}, f32[768,2]{0,1:T(2,128)}, u32[]{:S(2)}) copy-start(f32[768,2]{0,1:T(2,128)} %param.29) | copy-start | bytes 18436
  6.5 43.4 %copy-start.3 = (f32[768,4]{0,1:T(4,128)S(1)}, f32[768,4]{0,1:T(4,128)}, u32[]{:S(2)}) copy-start(f32[768,4]{0,1:T(4,128)} %param.25) | copy-start | bytes 36868
  6.5 74.7 %all-gather.12.cloned.1.call-start = ((), (), s32[]{:S(2)}) async-start(), calls=%async_computation.2 | async-start | bytes 3538944 | tf_op jit(solution)/shard_map/all_gather | solution.py:102
  8.5 248.5 %copy-start.10 = (bf16[768,256]{1,0:T(8,128)(2,1)S(1)}, bf16[768,256]{1,0:T(8,128)(2,1)}, u32[]{:S(2)}) copy-start(bf16[768,256]{1,0:T(8,128)(2,1)} %param.26) | copy-start | bytes 1179652
  8.5 126.5 %all-gather.14.cloned.1.call-start = ((), (), s32[]{:S(2)}) async-start(), calls=%async_computation.3 | async-start | bytes 3538944 | tf_op jit(solution)/shard_map/all_gather | solution.py:103
  10.6 185.4 %all-gather.16.cloned.1.call-start = ((), (), s32[]{:S(2)}) async-start(), calls=%async_computation.4 | async-start | bytes 3538944 | tf_op jit(solution)/shard_map/all_gather | solution.py:104
  12.6 244.2 %all-gather.18.cloned.1.call-start = ((), (), s32[]{:S(2)}) async-start(), calls=%async_computation.5 | async-start | bytes 3538944 | tf_op jit(solution)/shard_map/all_gather | solution.py:105
  14.6 283.6 %all-gather.20.cloned.1.call-start = ((), (), s32[]{:S(2)}) async-start(), calls=%async_computation.6 | async-start | bytes 5242880 | tf_op jit(solution)/shard_map/all_gather | solution.py:171
  15.2 312.8 %all-gather.22.cloned.1.call-start = ((), (), s32[]{:S(2)}) async-start(), calls=%async_computation.7 | async-start | bytes 5242880 | tf_op jit(solution)/shard_map/all_gather | solution.py:175
  15.8 410.9 %all-gather.26.cloned.1.call-start = ((), (), s32[]{:S(2)}) async-start(), calls=%async_computation.9 | async-start | bytes 6488064 | tf_op jit(solution)/shard_map/all_gather | solution.py:191
  16.5 440.9 %all-gather.24.cloned.1.call-start = ((), (), s32[]{:S(2)}) async-start(), calls=%async_computation.8 | async-start | bytes 3932160 | tf_op jit(solution)/shard_map/all_gather | solution.py:181
  328.0 3.9 copy-start.6
  333.2 218.8 %all-gather.28.cloned.1.call-start = ((), (), s32[]{:S(2)}) async-start(), calls=%async_computation.10 | async-start | bytes 6488064 | tf_op jit(solution)/shard_map/all_gather | solution.py:192
  333.9 310.8 %all-gather.30.cloned.1.call-start = ((), (), s32[]{:S(2)}) async-start(), calls=%async_computation.12 | async-start | bytes 6488064 | tf_op jit(solution)/shard_map/all_gather | solution.py:217
  334.5 379.1 %reduce-scatter.2.cloned.1.call-start = ((), (), s32[]{:S(2)}) async-start(), calls=%async_computation.11 | async-start | bytes 3932160 | tf_op jit(solution)/shard_map/reduce_scatter | solution.py:220
  465.8 1.4 copy-start.1
  467.2 97.0 %copy-start.7 = (f32[3,1408]{1,0:T(4,128)S(1)}, f32[3,1408]{1,0:T(4,128)}, u32[]{:S(2)}) copy-start(f32[3,1408]{1,0:T(4,128)} %param.36) | copy-start | bytes 50692
  467.2 97.0 %copy-start.8 = (f32[3,1408]{1,0:T(4,128)S(1)}, f32[3,1408]{1,0:T(4,128)}, u32[]{:S(2)}) copy-start(f32[3,1408]{1,0:T(4,128)} %param.37) | copy-start | bytes 50692
  560.3 1.3 copy-start.2
  561.7 91.3 %collective-permute-start = (bf16[2,2816]{1,0:T(2,128)(2,1)S(1)}, bf16[2,2816]{1,0:T(2,128)(2,1)S(1)}, u32[]{:S(2)}, u32[]{:S(2)}) collective-permute-start(bf16[2,2816]{1,0:T(2,128)(2,1)S(1)} %pad_maximum_fusion.1), channel_id=1, source_target_pairs={{0,4},{4,8},{8,12},{12,16},{16,20},{20,24},{24,28},{1,5},{5,9},{9,... | collective-permute-start | bytes 33800 | tf_op jit(solution)/shard_map/ppermute | solution.py:16
  677.3 39.7 %copy-start.9 = (f32[2048]{0:T(1024)S(1)}, f32[2048]{0:T(1024)}, u32[]{:S(2)}) copy-start(f32[2048]{0:T(1024)} %param.39) | copy-start | bytes 24580
  713.6 3.5 copy-start
Sparse Core Ops, SparseCore 0:
  9.6 64.2 all-gather.11
  76.1 58.8 all-gather.13
  137.3 58.6 all-gather.15
  198.1 58.6 all-gather.17
  258.2 37.8 all-gather.19
  297.5 30.4 all-gather.21
  330.2 96.3 all-gather.25
  428.2 29.1 all-gather.23
  459.6 92.2 all-gather.27
  554.0 90.7 all-gather.29
  677.5 36.0 reduce-scatter.1
